TPU v7x, 32 devices: a whole 2x2x4 slice. The times are simulated.
32 devices in a mesh: ep: 4 (over y, x), tp: 8 (over z, core).
Axes of the slice: x: 2, y: 2, z: 4, core: 2. Of those that a mesh axis runs over, the one named last changes fastest.
Arguments:
- queries: bfloat16 [2048, 16, 128], P('ep', 'tp'), may hold values from -125 to 125
- keys: bfloat16 [2048, 16, 128], P('ep', 'tp'), may hold values from -9 to 9
- values: bfloat16 [2048, 16, 128], P('ep', 'tp'), may hold values from -6 to 6
- mixing: float32 [16], P('tp'), may hold values from 0.3 to 0.8
- head_gain: float32 [128], replicated, may hold values from 0.1 to 1.9
- out_weight: bfloat16 [16, 128, 2048], P('tp'), may hold values from -0.125 to 0.125
- tokens_b: bfloat16 [4096, 2048], P(('ep', 'tp')), may hold values from -6 to 6
- norm_gain: float32 [2048], replicated, may hold values from 0.1 to 1.9
- expert_ids: int32 [4096, 2], P(('ep', 'tp')), may hold values from 0 to 3, all different within a row; in each aligned block of 128 rows (0 to 127, 128 to 255, ...) at most 96 rows name the same one
- group_gate: float32 [4096], P(('ep', 'tp')), may hold values from 0.2 to 1
- expert_gate: float32 [4096, 2], P(('ep', 'tp')), may hold values from 0.1 to 0.9
- gate_weight: bfloat16 [4, 2048, 1024], P('ep', None, 'tp'), may hold values from -0.125 to 0.125
- up_weight: bfloat16 [4, 2048, 1024], P('ep', None, 'tp'), may hold values from -0.125 to 0.125
- down_weight: bfloat16 [4, 2048, 1024], P('ep', None, 'tp'), may hold values from -0.1875 to 0.1875
Outputs:
- mixed: bfloat16 [2048, 2048], P(('ep', 'tp'))
- routed: bfloat16 [4096, 2048], P(('ep', 'tp'))
Inputs may be any that keep to these rules, and one draw needn't show every extreme that they name: `expert_ids`: within each aligned block of 128 rows, no expert is named by more than 96 rows, and some block has an expert named by exactly 96 rows.
All inputs are finite; a program needn't handle non-finite values.
Results may differ from a plain program's by a relative error of at most 0.019.
Values may be sent and summed in bfloat16 or wider, within the bound.
A program may use at most 192 MiB of HBM per device.

v0:
```python
import math
import jax
import jax.numpy as jnp
from jax import lax
from jax.sharding import PartitionSpec as P

HEAD = 64


def attend_heads(queries, keys, values, mixing, head_gain):
    shard_rows = queries.shape[0]
    head_count = queries.shape[1]
    value_width = values.shape[2]
    query_start = lax.axis_index("ep") * shard_rows
    score_scale = 1.0 / math.sqrt(HEAD)
    query_pos = query_start + lax.iota(jnp.int32, shard_rows)

    def update(running, key_block, value_block, block_start):
        key_pos = block_start + lax.iota(jnp.int32, shard_rows)
        allowed = key_pos[None, :] <= query_pos[:, None]
        fresh = []
        for map_index in range(2):
            maximum, row_sum, numerator = running[3 * map_index : 3 * map_index + 3]
            offset = map_index * HEAD
            scores = (
                jnp.einsum(
                    "qhd,khd->hqk",
                    queries[:, :, offset : offset + HEAD],
                    key_block[:, :, offset : offset + HEAD],
                    preferred_element_type=jnp.float32,
                )
                * score_scale
            )
            scores = jnp.where(allowed[None], scores, -1e30)
            newmax = jnp.maximum(maximum, jnp.max(scores, axis=2))
            shrink = jnp.exp(maximum - newmax)
            weights = jnp.exp(scores - newmax[:, :, None])
            row_sum = row_sum * shrink + jnp.sum(weights, axis=2)
            numerator = numerator * shrink[:, :, None] + jnp.einsum(
                "hqk,khe->hqe",
                weights.astype(jnp.bfloat16),
                value_block,
                preferred_element_type=jnp.float32,
            )
            fresh += [newmax, row_sum, numerator]
        return tuple(fresh)

    floor_max = jnp.full((head_count, shard_rows), -1e30, jnp.float32)
    zero_sum = jnp.zeros((head_count, shard_rows), jnp.float32)
    zero_acc = jnp.zeros((head_count, shard_rows, value_width), jnp.float32)
    start_state = (floor_max, zero_sum, zero_acc, floor_max, zero_sum, zero_acc)
    running = start_state
    key_piece = lax.all_gather(keys, "ep", axis=0, tiled=True)
    value_piece = lax.all_gather(values, "ep", axis=0, tiled=True)
    blocks = key_piece.shape[0] // shard_rows
    key_blocks = key_piece.reshape(blocks, shard_rows, head_count, key_piece.shape[2])
    value_blocks = value_piece.reshape(blocks, shard_rows, head_count, value_width)

    def visit_block(state, inputs):
        key_block, value_block, block_index = inputs
        block_start = block_index * shard_rows
        state = lax.cond(
            block_start <= query_start + shard_rows - 1,
            lambda state_in: update(state_in, key_block, value_block, block_start),
            lambda state_in: state_in,
            state,
        )
        return (state, None)

    running, unused = lax.scan(
        visit_block, running, (key_blocks, value_blocks, lax.iota(jnp.int32, blocks))
    )
    state = running
    diff = state[2] / state[1][:, :, None] - mixing[:, None, None] * state[5] / state[4][:, :, None]
    normed = diff * lax.rsqrt(jnp.mean(diff * diff, axis=2, keepdims=True) + 1e-05) * head_gain
    return normed.astype(jnp.bfloat16)


def mixer_half(queries, keys, values, mixing, head_gain, out_weight):
    attended = attend_heads(queries, keys, values, mixing, head_gain)
    return lax.psum_scatter(
        jnp.einsum("hqe,hed->qd", attended, out_weight, preferred_element_type=jnp.float32).astype(
            jnp.bfloat16
        ),
        "tp",
        scatter_dimension=0,
        tiled=True,
    )


def expert_half(
    tokens_b, norm_gain, expert_ids, group_gate, expert_gate, gate_weight, up_weight, down_weight
):
    local_rows = tokens_b.shape[0]
    width = tokens_b.shape[1]
    top_count = expert_ids.shape[1]
    ep_count = lax.axis_size("ep")
    local_count = gate_weight.shape[0]
    expert_total = ep_count * local_count
    capacity = 3 * local_rows * top_count // (2 * expert_total)
    tokens_f = tokens_b.astype(jnp.float32)
    normed = (
        tokens_f
        * lax.rsqrt(jnp.mean(tokens_f * tokens_f, axis=1, keepdims=True) + 1e-06)
        * norm_gain
    ).astype(jnp.bfloat16)
    flat_ids = expert_ids.reshape(-1)
    one_hot = (flat_ids[:, None] == lax.iota(jnp.int32, expert_total)[None, :]).astype(jnp.int32)
    slot_rank = jnp.sum((jnp.cumsum(one_hot, axis=0) - one_hot) * one_hot, axis=1)
    slot_index = flat_ids * capacity + slot_rank
    owners = jnp.full((expert_total * capacity,), local_rows, jnp.int32)
    owners = owners.at[slot_index].set(lax.iota(jnp.int32, local_rows * top_count) // top_count)
    padded = jnp.concatenate([normed, jnp.zeros((1, width), jnp.bfloat16)], axis=0)
    outgoing = padded[owners].reshape(ep_count, local_count * capacity, width)
    incoming = lax.all_to_all(outgoing, "ep", split_axis=0, concat_axis=0, tiled=True)
    expert_rows = jnp.transpose(
        incoming.reshape(ep_count, local_count, capacity, width), (1, 0, 2, 3)
    )
    expert_rows = expert_rows.reshape(local_count, ep_count * capacity, width)
    piece_gate = lax.all_gather(gate_weight, "tp", axis=2, tiled=True)
    piece_up = lax.all_gather(up_weight, "tp", axis=2, tiled=True)
    piece_down = lax.all_gather(down_weight, "tp", axis=2, tiled=True)
    gate_part = jnp.einsum(
        "jrd,jdf->jrf", expert_rows, piece_gate, preferred_element_type=jnp.float32
    )
    up_part = jnp.einsum("jrd,jdf->jrf", expert_rows, piece_up, preferred_element_type=jnp.float32)
    hidden = (jax.nn.silu(gate_part) * up_part).astype(jnp.bfloat16)
    expert_out = jnp.einsum(
        "jrf,jdf->jrd", hidden, piece_down, preferred_element_type=jnp.float32
    ).astype(jnp.bfloat16)
    outbound = jnp.transpose(
        expert_out.reshape(local_count, ep_count, capacity, width), (1, 0, 2, 3)
    )
    outbound = outbound.reshape(ep_count, local_count * capacity, width)
    returned = lax.all_to_all(outbound, "ep", split_axis=0, concat_axis=0, tiled=True).reshape(
        expert_total * capacity, width
    )
    picked = returned[slot_index].reshape(local_rows, top_count, width).astype(jnp.float32)
    route_weight = group_gate[:, None] * expert_gate
    return jnp.sum(route_weight[:, :, None] * picked, axis=1).astype(jnp.bfloat16)


def per_device(
    queries,
    keys,
    values,
    mixing,
    head_gain,
    out_weight,
    tokens_b,
    norm_gain,
    expert_ids,
    group_gate,
    expert_gate,
    gate_weight,
    up_weight,
    down_weight,
):
    mixed = mixer_half(queries, keys, values, mixing, head_gain, out_weight)
    routed = expert_half(
        tokens_b,
        norm_gain,
        expert_ids,
        group_gate,
        expert_gate,
        gate_weight,
        up_weight,
        down_weight,
    )
    return (mixed, routed)


def solution(mesh):
    placed = (
        P("ep", "tp", None),
        P("ep", "tp", None),
        P("ep", "tp", None),
        P("tp"),
        P(),
        P("tp", None, None),
        P(("ep", "tp"), None),
        P(),
        P(("ep", "tp"), None),
        P(("ep", "tp")),
        P(("ep", "tp"), None),
        P("ep", None, "tp"),
        P("ep", None, "tp"),
        P("ep", None, "tp"),
    )
    return jax.shard_map(
        per_device,
        mesh=mesh,
        in_specs=placed,
        out_specs=(P(("ep", "tp"), None), P(("ep", "tp"), None)),
        check_vma=False,
    )
```

profile of v0, /device:TPU:0, one launch (start us, length us, event | category | flops | bytes accessed | tf_op | source)
XLA Modules:
  0.0 260.2 jit_solution(6079203360803837472)
XLA Ops:
  7.3 1.8 copy.24
  9.1 1.7 copy.25
  10.9 0.7 all-gather.10.cloned.1.call-update
  13.4 1.2 reduce-window.6
  15.3 1.4 scatter_custom_fusion
  17.0 1.0 fusion.33
  17.9 21.8 %all-gather.6.cloned.1.call-done = bf16[2048,2,128]{2,0,1:T(8,128)(2,1)} async-done(((bf16[512,2,128]{2,0,1:T(8,128)(2,1)}), bf16[2048,2,128]{2,0,1:T(8,128)(2,1)}) %all-gather.6.cloned.1.call-update) | async-done | bytes 1048592 | tf_op jit(solution)/shard_map/all_gather | solution.py:53
  39.7 2.3 copy.26
  42.0 26.1 %all-gather.8.cloned.1.call-done = bf16[2048,2,128]{2,0,1:T(8,128)(2,1)} async-done(((bf16[512,2,128]{2,0,1:T(8,128)(2,1)}), bf16[2048,2,128]{2,0,1:T(8,128)(2,1)}) %all-gather.8.cloned.1.call-update) | async-done | bytes 1048592 | tf_op jit(solution)/shard_map/all_gather | solution.py:54
  68.1 1.3 copy.28
  69.5 9.8 %while.23 = (s32[]{:T(128)}, f32[2,512]{1,0:T(2,128)S(1)}, f32[2,512]{1,0:T(2,128)S(1)}, f32[2,512,128]{2,1,0:T(8,128)S(1)}, f32[2,512]{1,0:T(2,128)S(1)}, /*ind...) while((s32[]{:T(128)}, f32[2,512]{1,0:T(2,128)S(1)}, ...), condition=%wide.region_7.8_spmd.clone, body=%wide.region_0.7_spmd.clone.sunk | while | flops 410784768 | bytes 17183128 | solution.py:70
  69.6 0.6 dynamic_slice.36
  70.8 4.6 %conditional.3 = ((f32[2,512]{1,0:T(2,128)S(1)}, f32[2,512]{1,0:T(2,128)S(1)}, f32[2,512,128]{2,1,0:T(8,128)S(1)}, f32[2,512]{1,0:T(2,128)S(1)}, f32[2,512]{1,0:T(2,128)S(1)}, /*index=5*/f32[2,512,128]{2,1,0:T(8,128)S(1)})) conditional(s32[]{:T(128)} %convert_element_type.87, (f32[2,512]{1,0:T(2,128)S(1)}, f32[2,512]{1,0:T(2,128)S(1)}, ...), branch_computations={%region_1.1_spmd, %region_2.6_spmd} | conditional | flops 410784768 | bytes 17180748 | solution.py:62
  70.8 1.0 dynamic-slice_bitcast_fusion
  72.1 0.6 fusion.45
  73.0 0.6 fusion.46
  74.0 0.7 convolution_add_fusion
  74.7 0.7 convolution_add_fusion.1
  75.5 0.6 dynamic_slice.36
  76.8 0.6 dynamic_slice.36
  79.9 2.1 bitcast_convert_fusion
  82.2 2.5 gather_fusion
  84.6 36.1 %all_to_all.10 = bf16[4,96,2048]{2,1,0:T(8,128)(2,1)} all-to-all(bf16[4,96,2048]{2,1,0:T(8,128)(2,1)S(1)} %bitcast.62), channel_id=1, replica_groups=mesh['ep'=4,'tp'=8] {'ep'}, dimensions={0} | all-to-all | bytes 3145728 | tf_op jit(solution)/shard_map/all_to_all | solution.py:115
  120.7 5.7 %fusion.24 = f32[384,1024]{1,0:T(8,128)} fusion(bf16[384,2048]{1,0:T(8,128)(2,1)} %bitcast.63, bf16[1,2048,1024]{2,1,0:T(8,128)(2,1)} %all-gather.10.cloned.1.call-done), kind=kOutput, calls=%fused_computation.38 | convolution fusion | flops 1610612736 | bytes 7340032 | tf_op jit(solution)/shard_map/jrd,jdf->jrf/dot_general | solution.py:123
  126.4 38.6 %all-gather.12.cloned.1.call-done = bf16[1,2048,1024]{2,1,0:T(8,128)(2,1)} async-done(((bf16[1,2048,128]{2,1,0:T(8,128)(2,1)}), bf16[1,2048,1024]{2,1,0:T(8,128)(2,1)}) %all-gather.12.cloned.1.call-update) | async-done | bytes 4194320 | tf_op jit(solution)/shard_map/all_gather | solution.py:121
  165.0 47.5 %all-gather.14.cloned.1.call-done = bf16[1,2048,1024]{2,1,0:T(8,128)(2,1)} async-done(((bf16[1,2048,128]{2,1,0:T(8,128)(2,1)}), bf16[1,2048,1024]{2,1,0:T(8,128)(2,1)}) %all-gather.14.cloned.1.call-update) | async-done | bytes 4194320 | tf_op jit(solution)/shard_map/all_gather | solution.py:122
  212.5 8.6 %fusion.26 = bf16[384,2048]{1,0:T(8,128)(2,1)} fusion(bf16[1,2048,1024]{2,1,0:T(8,128)(2,1)} %all-gather.14.cloned.1.call-done, f32[384,1024]{1,0:T(8,128)} %fusion.24, bf16[384,2048]{1,0:T(8,128)(2,1)S(1)} %bitcast.64, bf16[1,2048,1024]{2,1,0:T(8,128)(2,1)} %all-gather.12.cloned.1.call-done), kind=kOutput, calls=%fused_computation.41 | convolution fusion | flops 3224371200 | bytes 13107200 | tf_op jit(solution)/shard_map/jrf,jdf->jrd/dot_general | solution.py:128
  221.1 3.8 %all-to-all-start.1 = ((bf16[4,96,2048]{2,1,0:T(8,128)(2,1)}), bf16[4,96,2048]{2,1,0:T(8,128)(2,1)S(1)}, u32[]{:S(2)}, u32[]{:S(2)}) async-start(bf16[4,96,2048]{2,1,0:T(8,128)(2,1)} %bitcast.65), calls=%async_computation.2 | async-start | bytes 3145728 | tf_op jit(solution)/shard_map/all_to_all | solution.py:135
  225.0 19.7 %all-to-all-done.1 = bf16[4,96,2048]{2,1,0:T(8,128)(2,1)S(1)} async-done(((bf16[4,96,2048]{2,1,0:T(8,128)(2,1)}), bf16[4,96,2048]{2,1,0:T(8,128)(2,1)S(1)}, u32[]{:S(2)}, u32[]{:S(2)}) %all-to-all-start.1) | async-done | bytes 1572896 | tf_op jit(solution)/shard_map/all_to_all | solution.py:135
  244.7 2.3 gather_fusion.1
  247.1 2.4 reshape.163
  249.4 3.9 %multiply_reduce_fusion = bf16[128,2048]{1,0:T(8,128)(2,1)} fusion(f32[128,2,2048]{2,1,0:T(2,128)S(1)} %reshape.163, f32[128,2]{1,0:T(8,128)S(1)} %copy.29), kind=kLoop, calls=%fused_computation.42 | loop fusion | flops 786432 | bytes 2622464 | tf_op jit(solution)/shard_map/reduce_sum | solution.py:140
  (87 shorter events, 5.1 us)
Async XLA Ops:
  7.2 72.7 %copy-start = (bf16[2,128,2048]{2,1,0:T(8,128)(2,1)S(1)}, bf16[2,128,2048]{2,1,0:T(8,128)(2,1)}, u32[]{:S(2)}) copy-start(bf16[2,128,2048]{2,1,0:T(8,128)(2,1)} %param.23) | copy-start | bytes 3145732
  7.2 5.6 %copy-start.6 = (s32[128,2]{0,1:T(2,128)S(1)}, s32[128,2]{0,1:T(2,128)}, u32[]{:S(2)}) copy-start(s32[128,2]{0,1:T(2,128)} %param.26) | copy-start | bytes 3076
  7.2 6.0 %copy-start.4 = (bf16[512,2,128]{2,1,0:T(2,128)(2,1)S(1)}, bf16[512,2,128]{2,1,0:T(2,128)(2,1)}, u32[]{:S(2)}) copy-start(bf16[512,2,128]{2,1,0:T(2,128)(2,1)} %param.18) | copy-start | bytes 786436
  7.2 9.5 %copy-start.1 = (bf16[128,2048]{1,0:T(8,128)(2,1)S(1)}, bf16[128,2048]{1,0:T(8,128)(2,1)}, u32[]{:S(2)}) copy-start(bf16[128,2048]{1,0:T(8,128)(2,1)} %param.24) | copy-start | bytes 1572868
  7.2 32.5 %all-gather.6.cloned.1.call-start = ((), (), s32[]{:S(2)}) async-start(), calls=%async_computation.3 | async-start | bytes 1310720 | tf_op jit(solution)/shard_map/all_gather | solution.py:53
  9.1 7.9 %copy-start.5 = (f32[2048]{0:T(1024)S(1)}, f32[2048]{0:T(1024)}, u32[]{:S(2)}) copy-start(f32[2048]{0:T(1024)} %param.25) | copy-start | bytes 24580
  9.1 59.0 %all-gather.8.cloned.1.call-start = ((), (), s32[]{:S(2)}) async-start(), calls=%async_computation.4 | async-start | bytes 1310720 | tf_op jit(solution)/shard_map/all_gather | solution.py:54
  10.8 109.8 %all-gather.10.cloned.1.call-start = ((), (), s32[]{:S(2)}) async-start(), calls=%async_computation.6 | async-start | bytes 4718592 | tf_op jit(solution)/shard_map/all_gather | solution.py:120
  11.6 153.4 %all-gather.12.cloned.1.call-start = ((), (), s32[]{:S(2)}) async-start(), calls=%async_computation.7 | async-start | bytes 4718592 | tf_op jit(solution)/shard_map/all_gather | solution.py:121
  12.2 200.3 %all-gather.14.cloned.1.call-start = ((), (), s32[]{:S(2)}) async-start(), calls=%async_computation.8 | async-start | bytes 4718592 | tf_op jit(solution)/shard_map/all_gather | solution.py:122
  12.7 240.6 %reduce-scatter.2.cloned.1.call-start = ((), (), s32[]{:S(2)}) async-start(), calls=%async_computation.5 | async-start | bytes 2359296 | tf_op jit(solution)/shard_map/reduce_scatter | solution.py:81
  69.5 9.9 %copy-start.8 = (f32[2]{0:T(128)S(1)}, f32[2]{0:T(128)}, u32[]{:S(2)}) copy-start(f32[2]{0:T(128)} %param.21) | copy-start | bytes 28
  69.5 10.4 %copy-start.9 = (f32[128]{0:T(128)S(1)}, f32[128]{0:T(128)}, u32[]{:S(2)}) copy-start(f32[128]{0:T(128)} %param.22) | copy-start | bytes 1540
  79.9 2.2 copy-start.2
  120.7 91.8 %copy-start.3 = (bf16[4,96,2048]{2,1,0:T(8,128)(2,1)S(1)}, bf16[4,96,2048]{2,1,0:T(8,128)(2,1)}, u32[]{:S(2)}) copy-start(bf16[4,96,2048]{2,1,0:T(8,128)(2,1)} %all_to_all.10) | copy-start | bytes 4718596
  221.1 3.8 %copy-start.7 = (f32[128,2]{0,1:T(2,128)S(1)}, f32[128,2]{0,1:T(2,128)}, u32[]{:S(2)}) copy-start(f32[128,2]{0,1:T(2,128)} %param.28) | copy-start | bytes 3076
  221.1 3.8 %copy-start.10 = (f32[128]{0:T(128)S(1)}, f32[128]{0:T(128)}, u32[]{:S(2)}) copy-start(f32[128]{0:T(128)} %param.27) | copy-start | bytes 1540
  221.1 23.6 %all-to-all-start.1 = ((bf16[4,96,2048]{2,1,0:T(8,128)(2,1)}), bf16[4,96,2048]{2,1,0:T(8,128)(2,1)S(1)}, u32[]{:S(2)}, u32[]{:S(2)}) async-start(bf16[4,96,2048]{2,1,0:T(8,128)(2,1)} %bitcast.65), calls=%async_computation.2 | async-start | bytes 3145728 | tf_op jit(solution)/shard_map/all_to_all | solution.py:135
Sparse Core Ops, SparseCore 0:
  10.4 29.2 all-gather.5
  41.5 26.4 all-gather.7
  69.7 47.8 all-gather.9
  119.0 45.9 all-gather.11
  166.4 45.9 all-gather.13
  215.2 34.1 reduce-scatter.1
where the time goes:
time: 261 us; the launch traced here: 260 us
  waiting for transfers between devices  155 us (59%)
  blocking collectives  36.1 us (14%)
  local copies, waits for them, and re-layouts  20.4 us (8%)
  matrix products  19.2 us (7%)
  between operations  14.4 us (6%)
  other arithmetic  7.89 us (3%)
  starting transfers between devices  4.02 us (2%)
  loops' own time  2.93 us (1%)
    all_gather x1, waiting for transfers between devices, expert_half(): piece_down = lax.all_gather(down_weight, 'tp', axis=2, tiled=True)  47.5 us
    all_gather x1, waiting for transfers between devices, expert_half(): piece_up = lax.all_gather(up_weight, 'tp', axis=2, tiled=True)  38.6 us
    all_to_all x1, blocking collectives, expert_half(): lax.all_to_all(outgoing, 'ep', split_axis=0, concat_axis=0, tiled=True)  36.1 us
    all_gather x1, waiting for transfers between devices, attend_heads(): value_piece = lax.all_gather(values, 'ep', axis=0, tiled=True)  26.1 us
    all_gather x1, waiting for transfers between devices, attend_heads(): key_piece = lax.all_gather(keys, 'ep', axis=0, tiled=True)  21.8 us
    all_to_all x1, waiting for transfers between devices, expert_half(): lax.all_to_all(outbound, 'ep', split_axis=0, concat_axis=0, tiled=True)  19.7 us
    dot_general x1, matrix products, expert_half(): jnp.einsum('jrf,jdf->jrd', hidden, piece_down, preferred_element_type=jnp...  8.63 us
    unnamed x28, local copies, waits for them, and re-layouts  7.42 us
  transfers between devices with their start and end apart: 7, of which 5 were waited for; matrix products, arithmetic and copies ran while one was open for 18% of the time, Pallas kernels for 0%

commit v1 on v0

--- a/solution.py
+++ b/solution.py
@@ -5,6 +5,30 @@
 from jax.sharding import PartitionSpec as P
 
 HEAD = 64
+
+
+def work_both_ways(value, axis, dim, work, out_dim):
+    size, index, extent = (lax.axis_size(axis), lax.axis_index(axis), value.shape[dim])
+    ahead = [(i, (i + 1) % size) for i in range(size)]
+    left = [(b, a) for a, b in ahead]
+    lower, upper = (lax.ppermute(value, axis, ahead), lax.ppermute(value, axis, left))
+    made = work(value, index * extent)
+    length = made.shape[out_dim]
+    out = jnp.zeros((*made.shape[:out_dim], size * length, *made.shape[out_dim + 1 :]), made.dtype)
+
+    def put(out, made, source):
+        return lax.dynamic_update_slice_in_dim(out, made, source * length, axis=out_dim)
+
+    out = put(out, made, index)
+    for step in range(1, size // 2 + 1):
+        below, above = ((index - step) % size, (index + step) % size)
+        current = (lower, upper)
+        if step < size // 2:
+            lower, upper = (lax.ppermute(lower, axis, ahead), lax.ppermute(upper, axis, left))
+        out = put(out, work(current[0], below * extent), below)
+        if 2 * step < size:
+            out = put(out, work(current[1], above * extent), above)
+    return out
 
 
 def attend_heads(queries, keys, values, mixing, head_gain):
@@ -118,12 +142,19 @@
     )
     expert_rows = expert_rows.reshape(local_count, ep_count * capacity, width)
     piece_gate = lax.all_gather(gate_weight, "tp", axis=2, tiled=True)
-    piece_up = lax.all_gather(up_weight, "tp", axis=2, tiled=True)
     piece_down = lax.all_gather(down_weight, "tp", axis=2, tiled=True)
     gate_part = jnp.einsum(
         "jrd,jdf->jrf", expert_rows, piece_gate, preferred_element_type=jnp.float32
     )
-    up_part = jnp.einsum("jrd,jdf->jrf", expert_rows, piece_up, preferred_element_type=jnp.float32)
+    up_part = work_both_ways(
+        up_weight,
+        "tp",
+        2,
+        lambda shard, start: jnp.einsum(
+            "jrd,jdf->jrf", expert_rows, shard, preferred_element_type=jnp.float32
+        ),
+        2,
+    )
     hidden = (jax.nn.silu(gate_part) * up_part).astype(jnp.bfloat16)
     expert_out = jnp.einsum(
         "jrf,jdf->jrd", hidden, piece_down, preferred_element_type=jnp.float32

time: 261 us -> 231 us (0.89)
  blocking collectives: 36.1 us -> 0 us
  waiting for transfers between devices: 155 us -> 127 us
  starting transfers between devices: 4.02 us -> 19.9 us
  matrix products: 19.2 us -> 29.8 us
  local copies, waits for them, and re-layouts: 20.4 us -> 27.1 us
    all_gather x1, waiting for transfers between devices: 0.01 us -> 46 us  [expert_half(): piece_gate = lax.all_gather(gate_weight, 'tp', axis=2, tiled=True)]
    all_gather x1, waiting for transfers between devices: 47.5 us -> 4.85 us  [expert_half(): piece_down = lax.all_gather(down_weight, 'tp', axis=2, tiled=True)]
    all_gather x1 -> x0, waiting for transfers between devices: 38.6 us -> none  [expert_half(): piece_up = lax.all_gather(up_weight, 'tp', axis=2, tiled=True)]
    ppermute x0 -> x7, waiting for transfers between devices: none -> 37.1 us  [the longest x3 26.6 us: work_both_ways(): lax.ppermute(lower, axis, ahead)]
    all_to_all x1 -> x0, blocking collectives: 36.1 us -> none  [expert_half(): lax.all_to_all(outgoing, 'ep', split_axis=0, concat_axis=0, tiled=True)]
    all_gather x1, waiting for transfers between devices: 21.8 us -> 0.01 us  [attend_heads(): key_piece = lax.all_gather(keys, 'ep', axis=0, tiled=True)]
    dot_general x1 -> x8, matrix products: 5.74 us -> 16.4 us  [expert_half(): jnp.einsum('jrd,jdf->jrf', expert_rows, shard, preferred_element_type=jnp...]
    ppermute x0 -> x7, starting transfers between devices: none -> 10.7 us  [the longest x2 7.08 us: work_both_ways(): lax.ppermute(upper, axis, left)]
  transfers between devices with their start and end apart: 7 -> 14, of which waited for: 5 -> 7; matrix products, arithmetic and copies ran while one was open for 18% -> 28% of each run, Pallas kernels for 0% -> 0%
where the time goes in v1:
time: 231 us; the launch traced here: 230 us
  waiting for transfers between devices  127 us (55%)
  matrix products  29.8 us (13%)
  local copies, waits for them, and re-layouts  27.1 us (12%)
  starting transfers between devices  19.9 us (9%)
  between operations  14 us (6%)
  other arithmetic  9.8 us (4%)
  loops' own time  2.9 us (1%)
    all_gather x1, waiting for transfers between devices, expert_half(): piece_gate = lax.all_gather(gate_weight, 'tp', axis=2, tiled=True)  46 us
    ppermute x3, waiting for transfers between devices, work_both_ways(): lax.ppermute(lower, axis, ahead)  26.6 us
    all_to_all x1, waiting for transfers between devices, expert_half(): lax.all_to_all(outbound, 'ep', split_axis=0, concat_axis=0, tiled=True)  19.7 us
    all_gather x1, waiting for transfers between devices, attend_heads(): value_piece = lax.all_gather(values, 'ep', axis=0, tiled=True)  17.9 us
    dot_general x8, matrix products, expert_half(): jnp.einsum('jrd,jdf->jrf', expert_rows, shard, preferred_element_type=jnp...  16.4 us
    ppermute x1, waiting for transfers between devices, work_both_ways(): lax.ppermute(value, axis, ahead)  10.5 us
    unnamed x28, local copies, waits for them, and re-layouts  9.17 us
    dot_general x1, matrix products, expert_half(): jnp.einsum('jrf,jdf->jrd', hidden, piece_down, preferred_element_type=jnp...  8.58 us
  transfers between devices with their start and end apart: 14, of which 7 were waited for; matrix products, arithmetic and copies ran while one was open for 28% of the time, Pallas kernels for 0%

profile of v1, /device:TPU:0, one launch (start us, length us, event | category | flops | bytes accessed | tf_op | source)
XLA Modules:
  0.0 230.3 jit_solution(11280290162226269101)
XLA Ops:
  7.2 1.8 copy.24
  9.1 1.7 copy.25
  15.0 1.4 scatter_custom_fusion
  16.4 3.1 %gather_fusion = bf16[384,2048]{1,0:T(8,128)(2,1)} fusion(bf16[129,2048]{1,0:T(8,128)(2,1)S(1)} %concatenate.3, s32[1024]{0:T(1024)S(1)} %pad_clamp_fusion.1), kind=kCustom, calls=%fused_computation | custom fusion | bytes 3147264 | tf_op jit(solution)/shard_map/gather | solution.py:138
  19.5 5.3 %all-to-all-start = ((bf16[4,96,2048]{2,1,0:T(8,128)(2,1)}), bf16[4,96,2048]{2,1,0:T(8,128)(2,1)S(1)}, u32[]{:S(2)}, u32[]{:S(2)}) async-start(bf16[4,96,2048]{2,1,0:T(8,128)(2,1)} %bitcast.145), calls=%async_computation.1 | async-start | bytes 3145728 | tf_op jit(solution)/shard_map/all_to_all | solution.py:139
  24.9 3.5 %collective-permute-start.1 = (bf16[1,2048,128]{2,1,0:T(8,128)(2,1)S(1)}, bf16[1,2048,128]{2,1,0:T(8,128)(2,1)}, u32[]{:S(2)}, u32[]{:S(2)}) collective-permute-start(bf16[1,2048,128]{2,1,0:T(8,128)(2,1)S(1)} %copy-done.5), channel_id=1, source_target_pairs={{1,0},{2,1},{3,2},{4,3},{5,4},{6,5},{7,6},{0,7},{9,8},{10,9},{11,1... | collective-permute-start | bytes 1572872 | tf_op jit(solution)/shard_map/ppermute | solution.py:14
  28.4 10.5 %collective-permute-done = bf16[1,2048,128]{2,1,0:T(8,128)(2,1)} collective-permute-done((bf16[1,2048,128]{2,1,0:T(8,128)(2,1)S(1)}, bf16[1,2048,128]{2,1,0:T(8,128)(2,1)}, u32[]{:S(2)}, u32[]{:S(2)}) %collective-permute-start) | collective-permute-done | bytes 524320 | tf_op jit(solution)/shard_map/ppermute | solution.py:14
  38.9 3.5 %collective-permute-start.3 = (bf16[1,2048,128]{2,1,0:T(8,128)(2,1)}, bf16[1,2048,128]{2,1,0:T(8,128)(2,1)}, u32[]{:S(2)}, u32[]{:S(2)}) collective-permute-start(bf16[1,2048,128]{2,1,0:T(8,128)(2,1)} %collective-permute-done.1), channel_id=1, source_target_pairs={{1,0},{2,1},{3,2},{4,3},{5,4},{6,5},{7,6},{0,7},{9,8},{10,9},{11,1... | collective-permute-start | bytes 1572872 | tf_op jit(solution)/shard_map/ppermute | solution.py:27
  43.3 9.5 %collective-permute-done.2 = bf16[1,2048,128]{2,1,0:T(8,128)(2,1)} collective-permute-done((bf16[1,2048,128]{2,1,0:T(8,128)(2,1)}, bf16[1,2048,128]{2,1,0:T(8,128)(2,1)}, u32[]{:S(2)}, u32[]{:S(2)}) %collective-permute-start.2) | collective-permute-done | bytes 524320 | tf_op jit(solution)/shard_map/ppermute | solution.py:27
  52.8 3.5 %collective-permute-start.5 = (bf16[1,2048,128]{2,1,0:T(8,128)(2,1)}, bf16[1,2048,128]{2,1,0:T(8,128)(2,1)}, u32[]{:S(2)}, u32[]{:S(2)}) collective-permute-start(bf16[1,2048,128]{2,1,0:T(8,128)(2,1)} %collective-permute-done.3), channel_id=1, source_target_pairs={{1,0},{2,1},{3,2},{4,3},{5,4},{6,5},{7,6},{0,7},{9,8},{10,9},{11,1... | collective-permute-start | bytes 1572872 | tf_op jit(solution)/shard_map/ppermute | solution.py:27
  59.0 2.3 %copy.26 = bf16[4,512,2,128]{1,3,2,0:T(8,128)(2,1)} copy(bf16[4,512,2,128]{3,1,0,2:T(8,128)(2,1)} %bitcast.147) | data formatting | bytes 2097152
  61.4 17.9 %all-gather.7.cloned.1.call-done = bf16[2048,2,128]{2,0,1:T(8,128)(2,1)} async-done(((bf16[512,2,128]{2,0,1:T(8,128)(2,1)}), bf16[2048,2,128]{2,0,1:T(8,128)(2,1)}) %all-gather.7.cloned.1.call-update) | async-done | bytes 1048592 | tf_op jit(solution)/shard_map/all_gather | solution.py:78
  79.3 2.3 %copy.28 = bf16[4,512,2,128]{3,1,2,0:T(8,128)(2,1)} copy(bf16[4,512,2,128]{3,1,0,2:T(8,128)(2,1)} %bitcast.148) | data formatting | bytes 2097152
  82.5 11.0 %while.23 = (s32[]{:T(128)}, f32[2,512]{1,0:T(2,128)S(1)}, f32[2,512]{1,0:T(2,128)S(1)}, f32[2,512,128]{2,1,0:T(8,128)S(1)}, f32[2,512]{1,0:T(2,128)S(1)}, /*ind...) while((s32[]{:T(128)}, f32[2,512]{1,0:T(2,128)S(1)}, ...), condition=%wide.region_7.8_spmd.clone, body=%wide.region_0.7_spmd.clone.sunk | while | flops 410784768 | bytes 25571820 | solution.py:94
  83.8 5.8 %conditional.3 = ((f32[2,512]{1,0:T(2,128)S(1)}, f32[2,512]{1,0:T(2,128)S(1)}, f32[2,512,128]{2,1,0:T(8,128)S(1)}, f32[2,512]{1,0:T(2,128)S(1)}, f32[2,512]{1,0:T(2,128)S(1)}, /*index=5*/f32[2,512,128]{2,1,0:T(8,128)})) conditional(s32[]{:T(128)} %convert_element_type.88, (f32[2,512]{1,0:T(2,128)S(1)}, f32[2,512]{1,0:T(2,128)S(1)}, ...), branch_computations={%region_1.1_spmd, %region_2.6_spmd} | conditional | flops 410784768 | bytes 25569440 | solution.py:86
  93.5 1.6 multiply_reduce_fusion.1
  95.1 2.1 bitcast_convert_fusion
  97.2 2.3 %fusion.39 = f32[1,384,1024]{2,1,0:T(8,128)} fusion(f32[1,384,1024]{2,1,0:T(8,128)} %fusion.40, s32[]{:T(128)S(6)} %select_n.90, bf16[384,2048]{1,0:T(8,128)(2,1)S(1)} %bitcast.136, bf16[1,2048,128]{2,1,0:T(8,128)(2,1)} %collective-permute-done), kind=kOutput, calls=%fused_computation.59 | convolution fusion | flops 201326592 | bytes 2293764 | tf_op jit(solution)/shard_map/jrd,jdf->jrf/dot_general | solution.py:153
  99.5 2.3 %fusion.38 = f32[1,384,1024]{2,1,0:T(8,128)} fusion(f32[1,384,1024]{2,1,0:T(8,128)} %fusion.39, s32[]{:T(128)S(6)} %select_n.92, bf16[384,2048]{1,0:T(8,128)(2,1)S(1)} %bitcast.137, bf16[1,2048,128]{2,1,0:T(8,128)(2,1)} %collective-permute-done.1), kind=kOutput, calls=%fused_computation.57 | convolution fusion | flops 201326592 | bytes 2293764 | tf_op jit(solution)/shard_map/jrd,jdf->jrf/dot_general | solution.py:153
  101.8 2.3 fusion.37
  104.1 2.3 %fusion.36 = f32[1,384,1024]{2,1,0:T(8,128)} fusion(f32[1,384,1024]{2,1,0:T(8,128)} %fusion.37, s32[]{:T(128)S(6)} %select_n.96, bf16[384,2048]{1,0:T(8,128)(2,1)S(1)} %bitcast.139, bf16[1,2048,128]{2,1,0:T(8,128)(2,1)} %collective-permute-done.3), kind=kOutput, calls=%fused_computation.53 | convolution fusion | flops 201326592 | bytes 2293764 | tf_op jit(solution)/shard_map/jrd,jdf->jrf/dot_general | solution.py:153
  106.4 2.3 %fusion.35 = f32[1,384,1024]{2,1,0:T(8,128)} fusion(f32[1,384,1024]{2,1,0:T(8,128)} %fusion.36, s32[]{:T(128)S(6)} %select_n.98, bf16[384,2048]{1,0:T(8,128)(2,1)S(1)} %bitcast.140, bf16[1,2048,128]{2,1,0:T(8,128)(2,1)} %collective-permute-done.4), kind=kOutput, calls=%fused_computation.51 | convolution fusion | flops 201326592 | bytes 2293764 | tf_op jit(solution)/shard_map/jrd,jdf->jrf/dot_general | solution.py:153
  108.8 2.3 %fusion.34 = f32[1,384,1024]{2,1,0:T(8,128)} fusion(f32[1,384,1024]{2,1,0:T(8,128)} %fusion.35, s32[]{:T(128)S(6)} %select_n.100, bf16[384,2048]{1,0:T(8,128)(2,1)S(1)} %bitcast.141, bf16[1,2048,128]{2,1,0:T(8,128)(2,1)} %collective-permute-done.5), kind=kOutput, calls=%fused_computation.49 | convolution fusion | flops 201326592 | bytes 2293764 | tf_op jit(solution)/shard_map/jrd,jdf->jrf/dot_general | solution.py:153
  111.1 17.1 %collective-permute-done.6 = bf16[1,2048,128]{2,1,0:T(8,128)(2,1)S(1)} collective-permute-done((bf16[1,2048,128]{2,1,0:T(8,128)(2,1)}, bf16[1,2048,128]{2,1,0:T(8,128)(2,1)S(1)}, u32[]{:S(2)}, u32[]{:S(2)}) %collective-permute-start.6) | collective-permute-done | bytes 524320 | tf_op jit(solution)/shard_map/ppermute | solution.py:27
  129.4 4.9 %all-gather.11.cloned.1.call-done = bf16[1,2048,1024]{2,1,0:T(8,128)(2,1)} async-done(((bf16[1,2048,128]{2,1,0:T(8,128)(2,1)}), bf16[1,2048,1024]{2,1,0:T(8,128)(2,1)}) %all-gather.11.cloned.1.call-update) | async-done | bytes 4194320 | tf_op jit(solution)/shard_map/all_gather | solution.py:145
  134.3 46.0 %all-gather.9.cloned.1.call-done = bf16[1,2048,1024]{2,1,0:T(8,128)(2,1)} async-done(((bf16[1,2048,128]{2,1,0:T(8,128)(2,1)}), bf16[1,2048,1024]{2,1,0:T(8,128)(2,1)}) %all-gather.9.cloned.1.call-update) | async-done | bytes 4194320 | tf_op jit(solution)/shard_map/all_gather | solution.py:144
  180.3 8.6 %fusion.24 = bf16[384,2048]{1,0:T(8,128)(2,1)} fusion(bf16[1,2048,1024]{2,1,0:T(8,128)(2,1)} %all-gather.11.cloned.1.call-done, f32[1,384,1024]{2,1,0:T(8,128)} %fusion.33, bf16[384,2048]{1,0:T(8,128)(2,1)S(1)} %bitcast.143, bf16[1,2048,1024]{2,1,0:T(8,128)(2,1)} %all-gather.9.cloned.1.call-done), kind=kOutput, calls=%fused_computation.39 | convolution fusion | flops 3224371200 | bytes 13107200 | tf_op jit(solution)/shard_map/jrf,jdf->jrd/dot_general | solution.py:159
  188.9 3.8 %all-to-all-start.1 = ((bf16[4,96,2048]{2,1,0:T(8,128)(2,1)}), bf16[4,96,2048]{2,1,0:T(8,128)(2,1)S(1)}, u32[]{:S(2)}, u32[]{:S(2)}) async-start(bf16[4,96,2048]{2,1,0:T(8,128)(2,1)} %bitcast.146), calls=%async_computation.2 | async-start | bytes 3145728 | tf_op jit(solution)/shard_map/all_to_all | solution.py:166
  192.8 19.7 %all-to-all-done.1 = bf16[4,96,2048]{2,1,0:T(8,128)(2,1)S(1)} async-done(((bf16[4,96,2048]{2,1,0:T(8,128)(2,1)}), bf16[4,96,2048]{2,1,0:T(8,128)(2,1)S(1)}, u32[]{:S(2)}, u32[]{:S(2)}) %all-to-all-start.1) | async-done | bytes 1572896 | tf_op jit(solution)/shard_map/all_to_all | solution.py:166
  212.5 2.3 %gather_fusion.1 = bf16[256,2048]{1,0:T(8,128)(2,1)} fusion(bf16[384,2048]{1,0:T(8,128)(2,1)S(1)} %bitcast.144, s32[1024]{0:T(1024)S(1)} %pad_clamp_fusion), kind=kCustom, calls=%fused_computation.1 | custom fusion | bytes 2098176 | tf_op jit(solution)/shard_map/gather | solution.py:169
  214.8 3.4 %reshape.212 = f32[128,2,2048]{2,1,0:T(2,128)} reshape(bf16[256,2048]{1,0:T(8,128)(2,1)} %gather_fusion.1) | data formatting | bytes 3145728 | tf_op jit(solution)/shard_map/convert_element_type | solution.py:169
  218.2 5.6 %multiply_reduce_fusion = bf16[128,2048]{1,0:T(8,128)(2,1)} fusion(f32[128,2,2048]{2,1,0:T(2,128)} %reshape.212, f32[128,2]{1,0:T(8,128)S(1)} %copy.29), kind=kLoop, calls=%fused_computation.40 | loop fusion | flops 786432 | bytes 2622464 | tf_op jit(solution)/shard_map/reduce_sum | solution.py:171
  (113 shorter events, 18.2 us)
Async XLA Ops:
  7.2 87.9 %copy-start = (bf16[2,128,2048]{2,1,0:T(8,128)(2,1)S(1)}, bf16[2,128,2048]{2,1,0:T(8,128)(2,1)}, u32[]{:S(2)}) copy-start(bf16[2,128,2048]{2,1,0:T(8,128)(2,1)} %param.23) | copy-start | bytes 3145732
  7.2 5.0 %copy-start.9 = (s32[128,2]{0,1:T(2,128)S(1)}, s32[128,2]{0,1:T(2,128)}, u32[]{:S(2)}) copy-start(s32[128,2]{0,1:T(2,128)} %param.26) | copy-start | bytes 3076
  7.2 7.2 %copy-start.4 = (bf16[128,2048]{1,0:T(8,128)(2,1)S(1)}, bf16[128,2048]{1,0:T(8,128)(2,1)}, u32[]{:S(2)}) copy-start(bf16[128,2048]{1,0:T(8,128)(2,1)} %param.24) | copy-start | bytes 1572868
  7.2 51.8 %all-gather.5.cloned.1.call-start = ((), (), s32[]{:S(2)}) async-start(), calls=%async_computation.3 | async-start | bytes 1310720 | tf_op jit(solution)/shard_map/all_gather | solution.py:77
  9.0 5.5 %copy-start.8 = (f32[2048]{0:T(1024)S(1)}, f32[2048]{0:T(1024)}, u32[]{:S(2)}) copy-start(f32[2048]{0:T(1024)} %param.25) | copy-start | bytes 24580
  9.1 70.2 %all-gather.7.cloned.1.call-start = ((), (), s32[]{:S(2)}) async-start(), calls=%async_computation.4 | async-start | bytes 1310720 | tf_op jit(solution)/shard_map/all_gather | solution.py:78
  10.8 123.5 %all-gather.11.cloned.1.call-start = ((), (), s32[]{:S(2)}) async-start(), calls=%async_computation.7 | async-start | bytes 4718592 | tf_op jit(solution)/shard_map/all_gather | solution.py:145
  11.6 168.7 %all-gather.9.cloned.1.call-start = ((), (), s32[]{:S(2)}) async-start(), calls=%async_computation.6 | async-start | bytes 4718592 | tf_op jit(solution)/shard_map/all_gather | solution.py:144
  19.5 5.3 %copy-start.5 = (bf16[1,2048,128]{2,1,0:T(8,128)(2,1)S(1)}, bf16[1,2048,128]{2,1,0:T(8,128)(2,1)}, u32[]{:S(2)}) copy-start(bf16[1,2048,128]{2,1,0:T(8,128)(2,1)} %param.30) | copy-start | bytes 1572868
  19.5 23.0 %copy-start.6 = (bf16[512,2,128]{2,1,0:T(2,128)(2,1)S(1)}, bf16[512,2,128]{2,1,0:T(2,128)(2,1)}, u32[]{:S(2)}) copy-start(bf16[512,2,128]{2,1,0:T(2,128)(2,1)} %param.18) | copy-start | bytes 786436
  19.5 36.9 %all-to-all-start = ((bf16[4,96,2048]{2,1,0:T(8,128)(2,1)}), bf16[4,96,2048]{2,1,0:T(8,128)(2,1)S(1)}, u32[]{:S(2)}, u32[]{:S(2)}) async-start(bf16[4,96,2048]{2,1,0:T(8,128)(2,1)} %bitcast.145), calls=%async_computation.1 | async-start | bytes 3145728 | tf_op jit(solution)/shard_map/all_to_all | solution.py:139
  24.8 198.9 %reduce-scatter.2.cloned.1.call-start = ((), (), s32[]{:S(2)}) async-start(), calls=%async_computation.5 | async-start | bytes 2359296 | tf_op jit(solution)/shard_map/reduce_scatter | solution.py:105
  24.8 14.1 %collective-permute-start = (bf16[1,2048,128]{2,1,0:T(8,128)(2,1)S(1)}, bf16[1,2048,128]{2,1,0:T(8,128)(2,1)}, u32[]{:S(2)}, u32[]{:S(2)}) collective-permute-start(bf16[1,2048,128]{2,1,0:T(8,128)(2,1)S(1)} %copy-done.5), channel_id=1, source_target_pairs={{0,1},{1,2},{2,3},{3,4},{4,5},{5,6},{6,7},{7,0},{8,9},{9,10},{10,1... | collective-permute-start | bytes 1572872 | tf_op jit(solution)/shard_map/ppermute | solution.py:14
  24.9 14.0 %collective-permute-start.1 = (bf16[1,2048,128]{2,1,0:T(8,128)(2,1)S(1)}, bf16[1,2048,128]{2,1,0:T(8,128)(2,1)}, u32[]{:S(2)}, u32[]{:S(2)}) collective-permute-start(bf16[1,2048,128]{2,1,0:T(8,128)(2,1)S(1)} %copy-done.5), channel_id=1, source_target_pairs={{1,0},{2,1},{3,2},{4,3},{5,4},{6,5},{7,6},{0,7},{9,8},{10,9},{11,1... | collective-permute-start | bytes 1572872 | tf_op jit(solution)/shard_map/ppermute | solution.py:14
  38.9 13.9 %collective-permute-start.2 = (bf16[1,2048,128]{2,1,0:T(8,128)(2,1)}, bf16[1,2048,128]{2,1,0:T(8,128)(2,1)}, u32[]{:S(2)}, u32[]{:S(2)}) collective-permute-start(bf16[1,2048,128]{2,1,0:T(8,128)(2,1)} %collective-permute-done), channel_id=1, source_target_pairs={{0,1},{1,2},{2,3},{3,4},{4,5},{5,6},{6,7},{7,0},{8,9},{9,10},{10,1... | collective-permute-start | bytes 1572872 | tf_op jit(solution)/shard_map/ppermute | solution.py:27
  38.9 13.9 %collective-permute-start.3 = (bf16[1,2048,128]{2,1,0:T(8,128)(2,1)}, bf16[1,2048,128]{2,1,0:T(8,128)(2,1)}, u32[]{:S(2)}, u32[]{:S(2)}) collective-permute-start(bf16[1,2048,128]{2,1,0:T(8,128)(2,1)} %collective-permute-done.1), channel_id=1, source_target_pairs={{1,0},{2,1},{3,2},{4,3},{5,4},{6,5},{7,6},{0,7},{9,8},{10,9},{11,1... | collective-permute-start | bytes 1572872 | tf_op jit(solution)/shard_map/ppermute | solution.py:27
  52.8 53.6 %collective-permute-start.4 = (bf16[1,2048,128]{2,1,0:T(8,128)(2,1)}, bf16[1,2048,128]{2,1,0:T(8,128)(2,1)}, u32[]{:S(2)}, u32[]{:S(2)}) collective-permute-start(bf16[1,2048,128]{2,1,0:T(8,128)(2,1)} %collective-permute-done.2), channel_id=1, source_target_pairs={{0,1},{1,2},{2,3},{3,4},{4,5},{5,6},{6,7},{7,0},{8,9},{9,10},{10,1... | collective-permute-start | bytes 1572872 | tf_op jit(solution)/shard_map/ppermute | solution.py:27
  52.8 55.9 %collective-permute-start.5 = (bf16[1,2048,128]{2,1,0:T(8,128)(2,1)}, bf16[1,2048,128]{2,1,0:T(8,128)(2,1)}, u32[]{:S(2)}, u32[]{:S(2)}) collective-permute-start(bf16[1,2048,128]{2,1,0:T(8,128)(2,1)} %collective-permute-done.3), channel_id=1, source_target_pairs={{1,0},{2,1},{3,2},{4,3},{5,4},{6,5},{7,6},{0,7},{9,8},{10,9},{11,1... | collective-permute-start | bytes 1572872 | tf_op jit(solution)/shard_map/ppermute | solution.py:27
  79.3 3.2 %copy-start.7 = (bf16[512,2,128]{0,2,1:T(8,128)(2,1)S(1)}, bf16[512,2,128]{0,2,1:T(8,128)(2,1)}, u32[]{:S(2)}) copy-start(bf16[512,2,128]{0,2,1:T(8,128)(2,1)} %copy.27) | copy-start | bytes 786436
  82.5 11.0 %copy-start.11 = (f32[2]{0:T(128)S(1)}, f32[2]{0:T(128)}, u32[]{:S(2)}) copy-start(f32[2]{0:T(128)} %param.21) | copy-start | bytes 28
  86.6 1.1 copy-start.1
  86.6 1.5 copy-start.3
  88.8 0.8 copy-start.2
  93.5 1.6 copy-start.12
  106.4 21.7 %collective-permute-start.6 = (bf16[1,2048,128]{2,1,0:T(8,128)(2,1)}, bf16[1,2048,128]{2,1,0:T(8,128)(2,1)S(1)}, u32[]{:S(2)}, u32[]{:S(2)}) collective-permute-start(bf16[1,2048,128]{2,1,0:T(8,128)(2,1)} %collective-permute-done.4), channel_id=1, source_target_pairs={{0,1},{1,2},{2,3},{3,4},{4,5},{5,6},{6,7},{7,0},{8,9},{9,10},{10,1... | collective-permute-start | bytes 1572872 | tf_op jit(solution)/shard_map/ppermute | solution.py:27
  188.9 3.8 %copy-start.10 = (f32[128,2]{0,1:T(2,128)S(1)}, f32[128,2]{0,1:T(2,128)}, u32[]{:S(2)}) copy-start(f32[128,2]{0,1:T(2,128)} %param.28) | copy-start | bytes 3076
  188.9 3.8 %copy-start.13 = (f32[128]{0:T(128)S(1)}, f32[128]{0:T(128)}, u32[]{:S(2)}) copy-start(f32[128]{0:T(128)} %param.27) | copy-start | bytes 1540
  188.9 23.6 %all-to-all-start.1 = ((bf16[4,96,2048]{2,1,0:T(8,128)(2,1)}), bf16[4,96,2048]{2,1,0:T(8,128)(2,1)S(1)}, u32[]{:S(2)}, u32[]{:S(2)}) async-start(bf16[4,96,2048]{2,1,0:T(8,128)(2,1)} %bitcast.146), calls=%async_computation.2 | async-start | bytes 3145728 | tf_op jit(solution)/shard_map/all_to_all | solution.py:166
Sparse Core Ops, SparseCore 0:
  10.4 37.6 all-gather.4
  50.6 28.6 all-gather.6
  80.9 53.3 all-gather.10
  135.7 44.5 all-gather.8
  183.0 34.2 reduce-scatter.1
